TPU v7x, 32 devices: a whole 2x2x4 slice. The times are simulated.
32 devices in a mesh: sp: 4 (over y, core), dp: 8 (over z, x).
Axes of the slice: x: 2, y: 2, z: 4, core: 2. Of those that a mesh axis runs over, the one named last changes fastest.
Arguments:
- stream: bfloat16 [8, 512, 2064], P('dp', 'sp'), may hold values from -6 to 6
- mix_gain: float32 [2064], replicated, may hold values from 0.1 to 1.9
- query_weight: bfloat16 [2064, 2048], P('dp'), may hold values from -0.125 to 0.125
- query_gain: float32 [128], replicated, may hold values from 0.1 to 1.9
- keys: bfloat16 [8, 512, 512], P('dp', 'sp'), may hold values from -6 to 6
- key_gain: float32 [128], replicated, may hold values from 0.1 to 1.9
- values: bfloat16 [8, 512, 512], P('dp', 'sp'), may hold values from -48 to 48
- stick_offset: float32 [16], replicated, may hold values from -8.5 to -7, as said below
Outputs:
- attended: bfloat16 [8, 512, 2048], P('dp', 'sp')
Inputs may be any that keep to these rules, and one draw needn't show every extreme that they name: `stick_offset`: one offset for each query head, added to all of that head's scores.
All inputs are finite; a program needn't handle non-finite values.
Results may differ from a plain program's by a relative error of at most 0.012.
Values may be sent and summed in bfloat16 or wider, within the bound.
A program may use at most 64 MiB of HBM per device.

v0:
```python
import math
import jax
import jax.numpy as jnp
from jax import lax
from jax.sharding import PartitionSpec as P

norm_eps = 1e-06
row_block = 256
key_block = 128


def rms_scaled(inputs, gain):
    wide = inputs.astype(jnp.float32)
    scaled = wide * lax.rsqrt(jnp.mean(wide * wide, axis=-1, keepdims=True) + norm_eps) * gain
    return scaled.astype(jnp.bfloat16)


def stick_weights(scores, first_row):
    heads_here = scores.shape[0]
    rows_here = scores.shape[1]
    keys_here = scores.shape[2]
    width = math.gcd(keys_here, key_block)
    blocks_here = keys_here // width
    query_pos = first_row + jnp.arange(rows_here, dtype=jnp.int32)
    key_pos = jnp.arange(keys_here, dtype=jnp.int32)
    causal = key_pos[None, :] < query_pos[:, None]
    log_keep = jnp.where(causal, jax.nn.log_sigmoid(-scores), 0.0)
    pieces = log_keep.reshape(heads_here, rows_here, blocks_here, width)
    inner = jnp.arange(width, dtype=jnp.int32)
    upper = (inner[:, None] > inner[None, :]).astype(jnp.float32)
    local = jnp.einsum("hqbk,kj->hqbj", pieces, upper, precision=lax.Precision.HIGHEST)
    totals = jnp.sum(pieces, axis=3)
    later = lax.cumsum(totals, axis=2, reverse=True) - totals
    tail = (local + later[:, :, :, None]).reshape(heads_here, rows_here, keys_here)
    return jnp.where(causal, jnp.exp(jax.nn.log_sigmoid(scores) + tail), 0.0)


def body(stream, mix_gain, query_weight, query_gain, keys, key_gain, values, stick_offset):
    sp_count = lax.axis_size("sp")
    sp_index = lax.axis_index("sp")
    stream_rows = stream[0]
    tokens_dev = stream_rows.shape[0]
    head_width = query_gain.shape[0]
    heads_all = stick_offset.shape[0]
    heads_dev = heads_all // sp_count
    kv_count = keys.shape[2] // head_width
    group_size = sp_count // kv_count
    seq_length = tokens_dev * sp_count
    stacked = jnp.stack((keys[0], values[0]), axis=1).reshape(tokens_dev, 2, kv_count, head_width)
    copied = jnp.repeat(stacked, group_size, axis=2)
    arrived = lax.all_to_all(copied, "sp", split_axis=2, concat_axis=0, tiled=True)
    key_value = arrived[:, :, 0, :]
    normed = rms_scaled(stream_rows, mix_gain)
    columns = lax.dynamic_slice_in_dim(
        query_weight, sp_index * (heads_dev * head_width), heads_dev * head_width, 1
    )
    gathered = lax.all_gather(columns, "dp", axis=0, tiled=True)
    queries = jnp.dot(
        lax.all_gather(normed, "sp", axis=0, tiled=True),
        gathered,
        preferred_element_type=jnp.float32,
    ).astype(jnp.bfloat16)
    queries = lax.optimization_barrier(queries)
    mine = rms_scaled(queries.reshape(seq_length, heads_dev, head_width), query_gain)
    key_heads = rms_scaled(key_value[:, 0], key_gain)
    value_rows = key_value[:, 1]
    offsets = lax.dynamic_slice_in_dim(stick_offset, sp_index * heads_dev, heads_dev)
    block = math.gcd(seq_length, row_block)
    outputs = []
    for block_id in range(seq_length // block):
        first = block_id * block
        finish = first + block
        scores = jnp.einsum(
            "qhd,kd->hqk",
            mine[first:finish],
            key_heads[:finish],
            preferred_element_type=jnp.float32,
        )
        scores = scores * head_width ** (-0.5) + offsets[:, None, None]
        weights = stick_weights(scores, first).astype(jnp.bfloat16)
        outputs.append(
            jnp.einsum(
                "hqk,kd->qhd", weights, value_rows[:finish], preferred_element_type=jnp.float32
            )
        )
    attended = (
        jnp.concatenate(outputs, axis=0)
        .reshape(seq_length, heads_dev * head_width)
        .astype(jnp.bfloat16)
    )
    returned = lax.all_to_all(attended, "sp", split_axis=0, concat_axis=1, tiled=True)
    return returned[None]


def solution(mesh):
    return jax.shard_map(
        body,
        mesh=mesh,
        in_specs=(
            P("dp", "sp", None),
            P(),
            P("dp", None),
            P(),
            P("dp", "sp", None),
            P(),
            P("dp", "sp", None),
            P(),
        ),
        out_specs=P("dp", "sp", None),
        check_vma=False,
    )
```

profile of v0, /device:TPU:0, one launch (start us, length us, event | category | flops | bytes accessed | tf_op | source)
XLA Modules:
  0.0 124.1 jit_solution(3568556610034957392)
XLA Ops:
  6.6 1.2 copy-done
  7.8 0.7 dynamic-slice_bitcast_fusion
  8.6 1.3 %fusion.15 = f32[128]{0:T(128)S(1)} fusion(bf16[1,128,2064]{1,2,0:T(8,128)(2,1)} %param.8), kind=kLoop, calls=%fused_computation.31 | loop fusion | flops 792448 | bytes 528896 | tf_op jit(solution)/shard_map/reduce_sum | solution.py:14
  9.9 2.2 %fusion.17 = bf16[128,2064]{0,1:T(8,128)(2,1)} fusion(bf16[1,128,2064]{1,2,0:T(8,128)(2,1)} %param.8, f32[2064]{0:T(1024)} %param.9, f32[128]{0:T(128)S(1)} %add_rsqrt_fusion.2), kind=kLoop, calls=%fused_computation.33 | loop fusion | flops 1056768 | bytes 1065536 | tf_op jit(solution)/shard_map/convert_element_type | solution.py:15
  12.5 0.9 copy.56
  13.3 4.3 %all-to-all-start = ((bf16[128,2,4,128]{3,0,1,2:T(8,128)(2,1)}), bf16[128,2,4,128]{3,0,1,2:T(8,128)(2,1)S(1)}, u32[]{:S(2)}, u32[]{:S(2)}) async-start(bf16[128,2,4,128]{3,0,1,2:T(8,128)(2,1)} %copy.56), calls=%async_computation | async-start | bytes 524288 | tf_op jit(solution)/shard_map/all_to_all | solution.py:51
  17.7 0.7 iota_compare_fusion
  18.5 5.2 %all-to-all-done = bf16[128,2,4,128]{3,0,1,2:T(8,128)(2,1)S(1)} async-done(((bf16[128,2,4,128]{3,0,1,2:T(8,128)(2,1)}), bf16[128,2,4,128]{3,0,1,2:T(8,128)(2,1)S(1)}, u32[]{:S(2)}, u32[]{:S(2)}) %all-to-all-start) | async-done | bytes 262176 | tf_op jit(solution)/shard_map/all_to_all | solution.py:51
  23.8 0.8 fusion.29
  24.6 37.5 %all-gather.6.cloned.1.call-done = bf16[8,258,512]{2,1,0:T(8,128)(2,1)} async-done(((bf16[1,258,512]{2,1,0:T(8,128)(2,1)}), bf16[8,258,512]{2,1,0:T(8,128)(2,1)}) %all-gather.6.cloned.1.call-update) | async-done | bytes 2113552 | tf_op jit(solution)/shard_map/all_gather | solution.py:57
  62.1 1.9 %reshape.90 = bf16[2064,512]{1,0:T(8,128)(2,1)S(1)} reshape(bf16[8,258,512]{2,1,0:T(8,128)(2,1)} %all-gather.6.cloned.1.call-done) | data formatting | bytes 4227072
  63.9 21.1 %all-gather.4.cloned.1.call-done = bf16[512,2064]{0,1:T(8,128)(2,1)} async-done(((bf16[128,2064]{0,1:T(8,128)(2,1)}), bf16[512,2064]{0,1:T(8,128)(2,1)}) %all-gather.4.cloned.1.call-update) | async-done | bytes 2113552 | tf_op jit(solution)/shard_map/all_gather | solution.py:59
  85.1 3.8 %convolution_convert_fusion = bf16[512,512]{1,0:T(8,128)(2,1)} fusion(bf16[512,2064]{0,1:T(8,128)(2,1)} %all-gather.4.cloned.1.call-done, bf16[2064,512]{1,0:T(8,128)(2,1)S(1)} %reshape.90), kind=kOutput, calls=%fused_computation.26 | convolution fusion | flops 1082392576 | bytes 4751360 | tf_op jit(solution)/shard_map/dot_general | solution.py:58
  88.9 1.4 %reshape.88 = f32[512,4,128]{2,1,0:T(4,128)S(1)} reshape(bf16[512,512]{1,0:T(8,128)(2,1)} %convolution_convert_fusion) | data formatting | bytes 1572864 | tf_op jit(solution)/shard_map/convert_element_type | solution.py:13
  91.4 0.8 copy-done.5
  92.2 1.8 %bitcast_reduce_fusion.1 = (f32[4,256,2]{1,2,0:T(2,128)S(1)}, f32[4,256,256]{1,2,0:T(8,128)S(1)}, f32[4,256,256]{1,2,0:T(8,128)S(1)}) fusion(pred[256,256]{0,1:T(8,128)(4,1)S(1)} %iota_compare_fusion.1, f32[4]{0:T(128)S(1)} %dynamic_slice.7, bf16[512,4,128]{2,0,1:T(8,128)(2,1)S(1)} %fusion.26, bf16[512,128]{1,0:T(8,128)(2,1)} %fusion.29), kind=kOutput, calls=%fused_computation.71 | convolution fusion | flops 69990400 | bytes 2499072 | tf_op jit(solution)/shard_map/qhd,kd->hqk/dot_general | solution.py:73
  94.1 0.7 convolution_add_fusion.1
  94.8 0.8 fusion.22
  95.6 1.0 fusion.13
  96.6 3.1 %bitcast_reduce_fusion = (f32[4,256,4]{1,2,0:T(4,128)S(1)}, f32[4,256,512]{1,2,0:T(8,128)}, f32[512,256,4]{1,0,2:T(8,128)S(1)}) fusion(f32[4]{0:T(128)S(1)} %dynamic_slice.7, pred[256,512]{0,1:T(8,128)(4,1)S(1)} %copy-done.3, bf16[512,4,128]{2,0,1:T(8,128)(2,1)S(1)} %copy-done.6, bf16[512,128]{1,0:T(8,128)(2,1)S(1)} %copy-done.9), kind=kOutput, calls=%fused_computation.70 | convolution fusion | flops 139980800 | bytes 4735488 | tf_op jit(solution)/shard_map/qhd,kd->hqk/dot_general | solution.py:73
  99.7 2.9 %convolution_add_fusion = f32[4,256,4,128]{1,3,2,0:T(8,128)S(1)} fusion(f32[4,256,4,128]{1,3,2,0:T(8,128)} %bitcast.99, f32[4,256,4]{1,2,0:T(4,128)S(1)} %sub.15), kind=kOutput, calls=%fused_computation.19 | convolution fusion | flops 805847040 | bytes 4210688 | tf_op jit(solution)/shard_map/hqbk,kj->hqbj/dot_general | solution.py:31
  102.6 1.8 %fusion.4 = bf16[4,256,512]{1,2,0:T(8,128)(2,1)S(1)} fusion(f32[4,256,4,128]{1,3,2,0:T(8,128)S(1)} %convolution_add_fusion, f32[512,256,4]{1,0,2:T(8,128)S(1)} %get-tuple-element.9, f32[4]{0:T(128)S(1)} %dynamic_slice.7, pred[256,512]{0,1:T(8,128)(4,1)S(1)} %copy-done.4), kind=kLoop, calls=%fused_computation.8 | loop fusion | flops 6815744 | bytes 5373968 | tf_op jit(solution)/shard_map/convert_element_type | solution.py:80
  105.0 11.2 %all_to_all.28 = bf16[4,128,512]{1,2,0:T(8,128)(2,1)S(1)} all-to-all(bf16[4,128,512]{1,2,0:T(8,128)(2,1)S(1)} %copy.66), channel_id=1, replica_groups=mesh['sp'=4,'dp'=8] {'sp'}, dimensions={0} | all-to-all | bytes 1048576 | tf_op jit(solution)/shard_map/all_to_all | solution.py:91
  116.2 1.0 copy.67
  (50 shorter events, 2.4 us)
Async XLA Ops:
  6.5 1.2 copy-start
  6.5 5.6 %copy-start.7 = (bf16[1,128,512]{2,1,0:T(8,128)(2,1)S(1)}, bf16[1,128,512]{2,1,0:T(8,128)(2,1)}, u32[]{:S(2)}) copy-start(bf16[1,128,512]{2,1,0:T(8,128)(2,1)} %param.12) | copy-start | bytes 393220
  6.5 5.8 %copy-start.8 = (bf16[1,128,512]{2,1,0:T(8,128)(2,1)S(1)}, bf16[1,128,512]{2,1,0:T(8,128)(2,1)}, u32[]{:S(2)}) copy-start(bf16[1,128,512]{2,1,0:T(8,128)(2,1)} %param.14) | copy-start | bytes 393220
  6.5 55.5 %all-gather.6.cloned.1.call-start = ((), (), s32[]{:S(2)}) async-start(), calls=%async_computation.3 | async-start | bytes 2433024 | tf_op jit(solution)/shard_map/all_gather | solution.py:57
  8.5 9.1 %copy-start.12 = (f32[16]{0:T(128)S(1)}, f32[16]{0:T(128)}, u32[]{:S(2)}) copy-start(f32[16]{0:T(128)} %param.15) | copy-start | bytes 196
  8.5 76.5 %all-gather.4.cloned.1.call-start = ((), (), s32[]{:S(2)}) async-start(), calls=%async_computation.2 | async-start | bytes 2641920 | tf_op jit(solution)/shard_map/all_gather | solution.py:59
  9.9 13.9 %copy-start.10 = (f32[128]{0:T(128)S(1)}, f32[128]{0:T(128)}, u32[]{:S(2)}) copy-start(f32[128]{0:T(128)} %param.13) | copy-start | bytes 1540
  13.3 10.3 %all-to-all-start = ((bf16[128,2,4,128]{3,0,1,2:T(8,128)(2,1)}), bf16[128,2,4,128]{3,0,1,2:T(8,128)(2,1)S(1)}, u32[]{:S(2)}, u32[]{:S(2)}) async-start(bf16[128,2,4,128]{3,0,1,2:T(8,128)(2,1)} %copy.56), calls=%async_computation | async-start | bytes 524288 | tf_op jit(solution)/shard_map/all_to_all | solution.py:51
  88.9 2.2 %copy-start.1 = (bf16[512,512]{1,0:T(8,128)(2,1)S(1)}, bf16[512,512]{1,0:T(8,128)(2,1)}, u32[]{:S(2)}) copy-start(bf16[512,512]{1,0:T(8,128)(2,1)} %convolution_convert_fusion) | copy-start | bytes 1572868
  88.9 2.2 %copy-start.11 = (f32[128]{0:T(128)S(1)}, f32[128]{0:T(128)}, u32[]{:S(2)}) copy-start(f32[128]{0:T(128)} %param.11) | copy-start | bytes 1540
  91.4 0.8 copy-start.5
  94.7 1.8 %copy-start.3 = (pred[256,512]{0,1:T(8,128)(4,1)S(1)}, pred[256,512]{0,1:T(8,128)(4,1)}, u32[]{:S(2)}) copy-start(pred[256,512]{0,1:T(8,128)(4,1)} %iota_compare_fusion) | copy-start | bytes 393220
  94.7 1.8 %copy-start.6 = (bf16[512,4,128]{2,0,1:T(8,128)(2,1)S(1)}, bf16[512,4,128]{2,0,1:T(8,128)(2,1)}, u32[]{:S(2)}) copy-start(bf16[512,4,128]{2,0,1:T(8,128)(2,1)} %copy-done.5) | copy-start | bytes 1572868
  94.8 1.8 %copy-start.9 = (bf16[512,128]{1,0:T(8,128)(2,1)S(1)}, bf16[512,128]{1,0:T(8,128)(2,1)}, u32[]{:S(2)}) copy-start(bf16[512,128]{1,0:T(8,128)(2,1)} %fusion.29) | copy-start | bytes 393220
  99.7 2.9 %copy-start.4 = (pred[256,512]{0,1:T(8,128)(4,1)S(1)}, pred[256,512]{0,1:T(8,128)(4,1)}, u32[]{:S(2)}) copy-start(pred[256,512]{0,1:T(8,128)(4,1)} %iota_compare_fusion) | copy-start | bytes 393220
  102.6 2.1 %copy-start.2 = (bf16[256,4,128]{0,2,1:T(8,128)(2,1)S(1)}, bf16[256,4,128]{0,2,1:T(8,128)(2,1)}, u32[]{:S(2)}) copy-start(bf16[256,4,128]{0,2,1:T(8,128)(2,1)} %fusion.13) | copy-start | bytes 786436
Sparse Core Ops, SparseCore 0:
  9.5 52.5 all-gather.5
  63.6 21.4 all-gather.3
where the time goes:
time: 125 us; the launch traced here: 124 us
  waiting for transfers between devices  63.8 us (51%)
  between operations  13.7 us (11%)
  matrix products  13.5 us (11%)
  blocking collectives  11.2 us (9%)
  other arithmetic  9.01 us (7%)
  local copies, waits for them, and re-layouts  8.58 us (7%)
  starting transfers between devices  4.31 us (3%)
    all_gather x1, waiting for transfers between devices, body(): gathered = lax.all_gather(columns, 'dp', axis=0, tiled=True)  37.5 us
    all_gather x1, waiting for transfers between devices, body(): lax.all_gather(normed, 'sp', axis=0, tiled=True)  21.1 us
    all_to_all x1, blocking collectives, body(): lax.all_to_all(attended, 'sp', split_axis=0, concat_axis=1, tiled=True)  11.2 us
    all_to_all x1, waiting for transfers between devices, body(): lax.all_to_all(copied, 'sp', split_axis=2, concat_axis=0, tiled=True)  5.16 us
    unnamed x30, local copies, waits for them, and re-layouts  4.87 us
    dot_general x2, matrix products, body(): jnp.einsum('qhd,kd->hqk', mine[first:finish], key_heads[:finish], preferr...  4.85 us
    all_to_all x1, starting transfers between devices, body(): lax.all_to_all(copied, 'sp', split_axis=2, concat_axis=0, tiled=True)  4.26 us
    dot_general x1, matrix products, body(): jnp.dot(lax.all_gather(normed, 'sp', axis=0, tiled=True), gathered, prefe...  3.8 us
  transfers between devices with their start and end apart: 3, of which 3 were waited for; matrix products, arithmetic and copies ran while one was open for 7% of the time, Pallas kernels for 0%

commit v1 on v0

--- a/solution.py
+++ b/solution.py
@@ -56,7 +56,9 @@
     )
     gathered = lax.all_gather(columns, "dp", axis=0, tiled=True)
     queries = jnp.dot(
-        lax.all_gather(normed, "sp", axis=0, tiled=True),
+        jnp.concatenate(
+            lax.all_to_all(jnp.stack([normed] * lax.axis_size("sp")), "sp", 0, 0), axis=0
+        ),
         gathered,
         preferred_element_type=jnp.float32,
     ).astype(jnp.bfloat16)

time: 125 us -> 104 us (0.83)
  waiting for transfers between devices: 63.8 us -> 35.8 us
  local copies, waits for them, and re-layouts: 8.58 us -> 16.3 us
  starting transfers between devices: 4.31 us -> 8.01 us
  other arithmetic: 9.01 us -> 5.43 us
    all_gather x1, waiting for transfers between devices: 37.5 us -> 6.4 us  [body(): gathered = lax.all_gather(columns, 'dp', axis=0, tiled=True)]
    all_to_all x0 -> x1, waiting for transfers between devices: none -> 24.1 us  [body(): lax.all_to_all(jnp.stack([normed] * lax.axis_size('sp')), 'sp', 0, 0)]
    all_gather x1 -> x0, waiting for transfers between devices: 21.1 us -> none  [body(): lax.all_gather(normed, 'sp', axis=0, tiled=True)]
    all_to_all x0 -> x1, starting transfers between devices: none -> 3.74 us  [body(): lax.all_to_all(jnp.stack([normed] * lax.axis_size('sp')), 'sp', 0, 0)]
    unnamed x30 -> x38, local copies, waits for them, and re-layouts: 4.87 us -> 8.27 us
    convert_element_type x3 -> x2, other arithmetic: 3.35 us -> 0.47 us  [rms_scaled(): return scaled.astype(jnp.bfloat16)]
    all_to_all x0 -> x1, local copies, waits for them, and re-layouts: none -> 2.72 us  [body(): lax.all_to_all(jnp.stack([normed] * lax.axis_size('sp')), 'sp', 0, 0)]
    another operation x0 -> x1, local copies, waits for them, and re-layouts: none -> 1.63 us  [body(): jnp.stack([normed] * lax.axis_size('sp'))]
  transfers between devices with their start and end apart: 3 -> 3, of which waited for: 3 -> 3; matrix products, arithmetic and copies ran while one was open for 7% -> 9% of each run, Pallas kernels for 0% -> 0%
where the time goes in v1:
time: 104 us; the launch traced here: 103 us
  waiting for transfers between devices  35.8 us (34%)
  local copies, waits for them, and re-layouts  16.3 us (16%)
  between operations  13.7 us (13%)
  matrix products  12.6 us (12%)
  blocking collectives  11.4 us (11%)
  starting transfers between devices  8.01 us (8%)
  other arithmetic  5.43 us (5%)
    all_to_all x1, waiting for transfers between devices, body(): lax.all_to_all(jnp.stack([normed] * lax.axis_size('sp')), 'sp', 0, 0)  24.1 us
    all_to_all x1, blocking collectives, body(): lax.all_to_all(attended, 'sp', split_axis=0, concat_axis=1, tiled=True)  11.4 us
    unnamed x38, local copies, waits for them, and re-layouts  8.27 us
    all_gather x1, waiting for transfers between devices, body(): gathered = lax.all_gather(columns, 'dp', axis=0, tiled=True)  6.4 us
    all_to_all x1, waiting for transfers between devices, body(): lax.all_to_all(copied, 'sp', split_axis=2, concat_axis=0, tiled=True)  5.36 us
    all_to_all x1, starting transfers between devices, body(): lax.all_to_all(copied, 'sp', split_axis=2, concat_axis=0, tiled=True)  4.26 us
    dot_general x2, matrix products, body(): jnp.einsum('qhd,kd->hqk', mine[first:finish], key_heads[:finish], preferr...  4.02 us
    dot_general x1, matrix products, body(): jnp.dot(jnp.concatenate(lax.all_to_all(jnp.stack([normed] * lax.axis_size...  3.77 us
  transfers between devices with their start and end apart: 3, of which 3 were waited for; matrix products, arithmetic and copies ran while one was open for 9% of the time, Pallas kernels for 0%

profile of v1, /device:TPU:0, one launch (start us, length us, event | category | flops | bytes accessed | tf_op | source)
XLA Modules:
  0.0 103.3 jit_solution(6314977315177437642)
XLA Ops:
  6.6 1.2 %copy-done = bf16[258,2048]{1,0:T(8,128)(2,1)S(1)} copy-done((bf16[258,2048]{1,0:T(8,128)(2,1)S(1)}, bf16[258,2048]{1,0:T(8,128)(2,1)}, u32[]{:S(2)}) %copy-start) | copy-done | bytes 1056792
  8.5 1.0 copy.57
  9.6 1.0 copy.58
  10.6 0.8 copy.59
  11.5 4.3 %all-to-all-start = ((bf16[128,2,4,128]{3,0,1,2:T(8,128)(2,1)}), bf16[128,2,4,128]{3,0,1,2:T(8,128)(2,1)S(1)}, u32[]{:S(2)}, u32[]{:S(2)}) async-start(bf16[128,2,4,128]{3,0,1,2:T(8,128)(2,1)} %copy.59), calls=%async_computation | async-start | bytes 524288 | tf_op jit(solution)/shard_map/all_to_all | solution.py:51
  16.4 5.4 %all-to-all-done = bf16[128,2,4,128]{3,0,1,2:T(8,128)(2,1)S(1)} async-done(((bf16[128,2,4,128]{3,0,1,2:T(8,128)(2,1)}), bf16[128,2,4,128]{3,0,1,2:T(8,128)(2,1)S(1)}, u32[]{:S(2)}, u32[]{:S(2)}) %all-to-all-start) | async-done | bytes 262176 | tf_op jit(solution)/shard_map/all_to_all | solution.py:51
  21.7 1.6 %stack.20 = bf16[4,128,2064]{1,2,0:T(8,128)(2,1)} broadcast(bf16[128,2064]{0,1:T(8,128)(2,1)S(1)} %fusion.27), dimensions={1,2} | broadcast | bytes 2641920 | tf_op jit(solution)/shard_map/stack | solution.py:60
  23.4 3.7 %all-to-all-start.1 = ((bf16[4,128,2064]{1,2,0:T(8,128)(2,1)}), bf16[4,128,2064]{1,2,0:T(8,128)(2,1)S(1)}, u32[]{:S(2)}, u32[]{:S(2)}) async-start(bf16[4,128,2064]{1,2,0:T(8,128)(2,1)} %stack.20), calls=%async_computation.1 | async-start | bytes 4227072 | tf_op jit(solution)/shard_map/all_to_all | solution.py:60
  27.3 0.7 iota_compare_fusion
  28.9 24.1 %all-to-all-done.1 = bf16[4,128,2064]{1,2,0:T(8,128)(2,1)S(1)} async-done(((bf16[4,128,2064]{1,2,0:T(8,128)(2,1)}), bf16[4,128,2064]{1,2,0:T(8,128)(2,1)S(1)}, u32[]{:S(2)}, u32[]{:S(2)}) %all-to-all-start.1) | async-done | bytes 2113568 | tf_op jit(solution)/shard_map/all_to_all | solution.py:60
  52.9 2.7 %copy.61 = bf16[4,128,2064]{2,1,0:T(8,128)(2,1)} copy(bf16[4,128,2064]{1,2,0:T(8,128)(2,1)S(1)} %all-to-all-done.1) | data formatting | bytes 4227072 | tf_op jit(solution)/shard_map/all_to_all | solution.py:60
  55.7 6.4 %all-gather.3.cloned.1.call-done = bf16[8,258,512]{2,1,0:T(8,128)(2,1)} async-done(((bf16[1,258,512]{2,1,0:T(8,128)(2,1)}), bf16[8,258,512]{2,1,0:T(8,128)(2,1)}) %all-gather.3.cloned.1.call-update) | async-done | bytes 2113552 | tf_op jit(solution)/shard_map/all_gather | solution.py:57
  62.1 2.9 %reshape.107 = bf16[2064,512]{1,0:T(8,128)(2,1)} reshape(bf16[8,258,512]{2,1,0:T(8,128)(2,1)} %all-gather.3.cloned.1.call-done) | data formatting | bytes 4227072
  65.0 3.8 %convolution_convert_fusion = bf16[512,512]{1,0:T(8,128)(2,1)} fusion(bf16[512,2064]{1,0:T(8,128)(2,1)S(1)} %bitcast.98, bf16[2064,512]{1,0:T(8,128)(2,1)} %reshape.107), kind=kOutput, calls=%fused_computation.26 | convolution fusion | flops 1082392576 | bytes 4751360 | tf_op jit(solution)/shard_map/dot_general | solution.py:58
  68.7 1.4 %reshape.105 = f32[512,4,128]{2,1,0:T(4,128)S(1)} reshape(bf16[512,512]{1,0:T(8,128)(2,1)} %convolution_convert_fusion) | data formatting | bytes 1572864 | tf_op jit(solution)/shard_map/convert_element_type | solution.py:13
  71.3 0.8 copy-done.9
  72.1 0.9 bitcast_reduce_fusion.1
  73.8 0.8 fusion.22
  74.6 1.0 fusion.13
  75.6 3.1 %bitcast_reduce_fusion = (f32[4,256,4]{1,2,0:T(4,128)S(1)}, f32[4,256,512]{1,2,0:T(8,128)}, f32[512,256,4]{1,0,2:T(8,128)S(1)}) fusion(f32[4]{0:T(128)S(1)} %dynamic_slice.7, pred[256,512]{0,1:T(8,128)(4,1)S(1)} %copy-done.7, bf16[512,4,128]{2,0,1:T(8,128)(2,1)S(1)} %copy-done.10, bf16[512,128]{1,0:T(8,128)(2,1)S(1)} %copy-done.12), kind=kOutput, calls=%fused_computation.71 | convolution fusion | flops 139980800 | bytes 4735488 | tf_op jit(solution)/shard_map/qhd,kd->hqk/dot_general | solution.py:75
  78.7 2.9 %convolution_add_fusion = f32[4,256,4,128]{1,3,2,0:T(8,128)S(1)} fusion(f32[4,256,4,128]{1,3,2,0:T(8,128)} %bitcast.99, f32[4,256,4]{1,2,0:T(4,128)S(1)} %sub.15), kind=kOutput, calls=%fused_computation.19 | convolution fusion | flops 805847040 | bytes 4210688 | tf_op jit(solution)/shard_map/hqbk,kj->hqbj/dot_general | solution.py:31
  81.6 1.8 %fusion.4 = bf16[4,256,512]{1,2,0:T(8,128)(2,1)S(1)} fusion(f32[4,256,4,128]{1,3,2,0:T(8,128)S(1)} %convolution_add_fusion, f32[512,256,4]{1,0,2:T(8,128)S(1)} %get-tuple-element.9, f32[4]{0:T(128)S(1)} %dynamic_slice.7, pred[256,512]{0,1:T(8,128)(4,1)S(1)} %copy-done.8), kind=kLoop, calls=%fused_computation.8 | loop fusion | flops 6815744 | bytes 5373968 | tf_op jit(solution)/shard_map/convert_element_type | solution.py:82
  84.0 11.4 %all_to_all.33 = bf16[4,128,512]{1,2,0:T(8,128)(2,1)S(1)} all-to-all(bf16[4,128,512]{1,2,0:T(8,128)(2,1)S(1)} %copy.70), channel_id=1, replica_groups=mesh['sp'=4,'dp'=8] {'sp'}, dimensions={0} | all-to-all | bytes 1048576 | tf_op jit(solution)/shard_map/all_to_all | solution.py:93
  95.4 1.0 copy.71
  (59 shorter events, 4.8 us)
Async XLA Ops:
  6.5 1.2 %copy-start = (bf16[258,2048]{1,0:T(8,128)(2,1)S(1)}, bf16[258,2048]{1,0:T(8,128)(2,1)}, u32[]{:S(2)}) copy-start(bf16[258,2048]{1,0:T(8,128)(2,1)} %param.10) | copy-start | bytes 3170308
  6.5 9.2 %copy-start.2 = (bf16[1,128,2064]{1,2,0:T(8,128)(2,1)S(1)}, bf16[1,128,2064]{1,2,0:T(8,128)(2,1)}, u32[]{:S(2)}) copy-start(bf16[1,128,2064]{1,2,0:T(8,128)(2,1)} %param.8) | copy-start | bytes 1585156
  6.5 9.5 %copy-start.13 = (f32[2064]{0:T(1024)S(1)}, f32[2064]{0:T(1024)}, u32[]{:S(2)}) copy-start(f32[2064]{0:T(1024)} %param.9) | copy-start | bytes 24772
  6.5 55.5 %all-gather.3.cloned.1.call-start = ((), (), s32[]{:S(2)}) async-start(), calls=%async_computation.3 | async-start | bytes 2433024 | tf_op jit(solution)/shard_map/all_gather | solution.py:57
  11.5 10.3 %all-to-all-start = ((bf16[128,2,4,128]{3,0,1,2:T(8,128)(2,1)}), bf16[128,2,4,128]{3,0,1,2:T(8,128)(2,1)S(1)}, u32[]{:S(2)}, u32[]{:S(2)}) async-start(bf16[128,2,4,128]{3,0,1,2:T(8,128)(2,1)} %copy.59), calls=%async_computation | async-start | bytes 524288 | tf_op jit(solution)/shard_map/all_to_all | solution.py:51
  23.4 3.8 %copy-start.16 = (f32[16]{0:T(128)S(1)}, f32[16]{0:T(128)}, u32[]{:S(2)}) copy-start(f32[16]{0:T(128)} %param.15) | copy-start | bytes 196
  23.4 5.4 %copy-start.14 = (f32[128]{0:T(128)S(1)}, f32[128]{0:T(128)}, u32[]{:S(2)}) copy-start(f32[128]{0:T(128)} %param.13) | copy-start | bytes 1540
  23.4 29.6 %all-to-all-start.1 = ((bf16[4,128,2064]{1,2,0:T(8,128)(2,1)}), bf16[4,128,2064]{1,2,0:T(8,128)(2,1)S(1)}, u32[]{:S(2)}, u32[]{:S(2)}) async-start(bf16[4,128,2064]{1,2,0:T(8,128)(2,1)} %stack.20), calls=%async_computation.1 | async-start | bytes 4227072 | tf_op jit(solution)/shard_map/all_to_all | solution.py:60
  28.0 0.7 copy-start.4
  28.9 42.4 %copy-start.11 = (bf16[512,128]{1,0:T(8,128)(2,1)}, bf16[512,128]{1,0:T(8,128)(2,1)S(1)}, u32[]{:S(2)}) copy-start(bf16[512,128]{1,0:T(8,128)(2,1)S(1)} %fusion.30) | copy-start | bytes 393220
  55.7 9.3 %copy-start.1 = (bf16[4,128,2064]{2,1,0:T(8,128)(2,1)S(1)}, bf16[4,128,2064]{2,1,0:T(8,128)(2,1)}, u32[]{:S(2)}) copy-start(bf16[4,128,2064]{2,1,0:T(8,128)(2,1)} %copy.61) | copy-start | bytes 6340612
  68.7 2.2 %copy-start.3 = (bf16[512,512]{1,0:T(8,128)(2,1)S(1)}, bf16[512,512]{1,0:T(8,128)(2,1)}, u32[]{:S(2)}) copy-start(bf16[512,512]{1,0:T(8,128)(2,1)} %convolution_convert_fusion) | copy-start | bytes 1572868
  68.7 2.2 %copy-start.15 = (f32[128]{0:T(128)S(1)}, f32[128]{0:T(128)}, u32[]{:S(2)}) copy-start(f32[128]{0:T(128)} %param.11) | copy-start | bytes 1540
  71.3 0.8 copy-start.9
  73.1 1.5 %copy-start.5 = (bf16[4,128,2,1,128]{4,1,0,2,3:T(8,128)(2,1)S(1)}, bf16[4,128,2,1,128]{4,1,0,2,3:T(8,128)(2,1)}, u32[]{:S(2)}) copy-start(bf16[4,128,2,1,128]{4,1,0,2,3:T(8,128)(2,1)} %copy-done.4) | copy-start | bytes 786436
  73.8 1.8 %copy-start.7 = (pred[256,512]{0,1:T(8,128)(4,1)S(1)}, pred[256,512]{0,1:T(8,128)(4,1)}, u32[]{:S(2)}) copy-start(pred[256,512]{0,1:T(8,128)(4,1)} %iota_compare_fusion) | copy-start | bytes 393220
  73.8 1.8 %copy-start.10 = (bf16[512,4,128]{2,0,1:T(8,128)(2,1)S(1)}, bf16[512,4,128]{2,0,1:T(8,128)(2,1)}, u32[]{:S(2)}) copy-start(bf16[512,4,128]{2,0,1:T(8,128)(2,1)} %copy-done.9) | copy-start | bytes 1572868
  73.8 1.8 %copy-start.12 = (bf16[512,128]{1,0:T(8,128)(2,1)S(1)}, bf16[512,128]{1,0:T(8,128)(2,1)}, u32[]{:S(2)}) copy-start(bf16[512,128]{1,0:T(8,128)(2,1)} %copy-done.11) | copy-start | bytes 393220
  78.7 2.9 %copy-start.8 = (pred[256,512]{0,1:T(8,128)(4,1)S(1)}, pred[256,512]{0,1:T(8,128)(4,1)}, u32[]{:S(2)}) copy-start(pred[256,512]{0,1:T(8,128)(4,1)} %iota_compare_fusion) | copy-start | bytes 393220
  81.6 2.2 %copy-start.6 = (bf16[256,4,128]{0,2,1:T(8,128)(2,1)S(1)}, bf16[256,4,128]{0,2,1:T(8,128)(2,1)}, u32[]{:S(2)}) copy-start(bf16[256,4,128]{0,2,1:T(8,128)(2,1)} %fusion.13) | copy-start | bytes 786436
Sparse Core Ops, SparseCore 0:
  9.5 52.5 all-gather.2
